TPU v7x, 32 devices: a whole 2x2x4 slice. The times are simulated.
32 devices in a mesh: rep: 2 (over x), fs: 4 (over z), tp: 4 (over y, core).
Axes of the slice: x: 2, y: 2, z: 4, core: 2. Of those that a mesh axis runs over, the one named last changes fastest.
Arguments:
- stream: bfloat16 [4096, 2048], P(('rep', 'fs', 'tp')), may hold values from -6 to 6
- gate_weight: bfloat16 [2048, 2816], P('fs', 'tp'), may hold values from -0.125 to 0.125
- up_weight: bfloat16 [2048, 2816], P('fs', 'tp'), may hold values from -0.125 to 0.125
- down_weight: bfloat16 [2816, 2048], P('tp', 'fs'), may hold values from -0.21875 to 0.21875
- query_weight: bfloat16 [2048, 512], P('fs', 'tp'), may hold values from -0.125 to 0.125
- key_weight: bfloat16 [2048, 512], P('fs', 'tp'), may hold values from -0.125 to 0.125
- value_weight: bfloat16 [2048, 1024], P('fs', 'tp'), may hold values from -0.125 to 0.125
- outgate_weight: bfloat16 [2048, 1024], P('fs', 'tp'), may hold values from -0.125 to 0.125
- decay_down: bfloat16 [2048, 32], replicated, may hold values from -0.125 to 0.125
- decay_up: bfloat16 [32, 512], P(None, 'tp'), may hold values from -2 to 2
- decay_bias: float32 [512], P('tp'), may hold values from -0.5 to 7
- head_gain: float32 [128], replicated, may hold values from 0.1 to 1.9
- out_weight: bfloat16 [1024, 2048], P('tp', 'fs'), may hold values from -0.375 to 0.375
- norm_gain: float32 [3, 2048], replicated, may hold values from 0.1 to 1.9
Outputs:
- layer_out: bfloat16 [4096, 2048], P(('rep', 'fs', 'tp'))
All inputs are finite; a program needn't handle non-finite values.
Results may differ from a plain program's by a relative error of at most 0.015.
Values may be sent and summed in bfloat16 or wider, within the bound.
A program may use at most 128 MiB of HBM per device.

v0:
```python
import functools

import jax
import jax.numpy as jnp
import numpy as np
from jax import lax
from jax.experimental import pallas as pl
from jax.experimental.pallas import tpu as pltpu
from jax.sharding import PartitionSpec as P

DK = 64
DV = 128
RESIDUAL_SCALE = 2.0**0.5
BRANCH_SCALE = 0.5
NORM_EPS = 1e-05
HEAD_EPS = 0.01
GATE_DIVISOR = 16.0
MESH = pl.DeviceIdType.MESH
CUTS = 2
AHEAD = 2
PARTS = 2
F32 = jnp.float32
BF16 = jnp.bfloat16
NT = (((1,), (1,)), ((), ()))
TN = (((0,), (0,)), ((), ()))


def level_tables(tile):
    row, col = np.arange(tile)[:, None], np.arange(tile)[None, :]
    sums, pairs = [], []
    half = 1
    while half < tile:
        start = row // half * half
        later = row // half % 2 == 1
        sums.append(
            np.where(later, (col >= start) & (col <= row), (col > row) & (col < start + half))
        )
        pairs.append(later & (col // half == row // half - 1))
        half *= 2
    sums += [col <= row, col > row]
    pairs.append(row == col)
    return (
        np.concatenate(sums, 0).astype(np.float32),
        np.concatenate(pairs, 0).astype(np.float32),
        len(pairs) - 1,
    )


def dot(a, b, dims=None):
    if dims is None:
        return jnp.dot(a, b, preferred_element_type=F32)
    return lax.dot_general(a, b, dims, preferred_element_type=F32)


def layer_kernel(
    sizes,
    levels,
    cuts,
    stream,
    gate_w,
    up_w,
    down_w,
    qkvg_w,
    out_w,
    decay_down,
    decay_up,
    decay_bias,
    head_gain,
    norm_gain,
    span_sums,
    pair_masks,
    result,
    gate_all,
    up_all,
    down_all,
    qkvg_all,
    out_all,
    rows_all,
    part_out,
    part_in,
    cross_out,
    cross_in,
    partial,
    gate_buf,
    hidden,
    proj,
    log_gate,
    gated,
    state,
    w_send,
    w_recv,
    ag_send,
    ag_recv,
    fwd_send,
    rs_send,
    rs_recv,
    cross_send,
    cross_recv,
):
    reps, shards, ranks, cores = sizes
    chips = ranks // cores
    rep, shard, rank = lax.axis_index("rep"), lax.axis_index("fs"), lax.axis_index("tp")
    chip, core = rank // cores, lax.rem(rank, cores)
    block, width = stream.shape
    length = block * ranks
    half_rows = chips * block
    partner = {"tp": chip * cores + (cores - 1 - core)}

    barrier = pltpu.get_barrier_semaphore()

    def greet(device):
        pl.semaphore_signal(barrier, inc=1, device_id=device, device_id_type=MESH)

    @pl.when(shard > 0)
    def _():
        greet({"fs": shard - 1})

    @pl.when(shard < shards - 1)
    def _():
        greet({"fs": shard + 1})

    for step in range(1, reps):
        greet({"rep": lax.rem(rep + step, reps)})
    for step in range(1, ranks):
        greet({"tp": lax.rem(rank + step, ranks)})
    neighbours = (
        jnp.where(shard > 0, 1, 0) + jnp.where(shard < shards - 1, 1, 0) + reps - 1 + ranks - 1
    )
    pl.semaphore_wait(barrier, neighbours)

    locals_ = (gate_w, up_w, down_w, qkvg_w, out_w)
    wholes = (gate_all, up_all, down_all, qkvg_all, out_all)

    def side_by_side(w):
        return wholes[w].shape[0] == locals_[w].shape[0]

    def piece(item, owner, part):
        w, cut = item // cuts, item % cuts
        rows, columns = locals_[w].shape
        size = rows // (reps * cuts)
        start = (part * cuts + cut) * size
        if side_by_side(w):
            return wholes[w].at[
                pl.ds(pl.multiple_of(start, size), size),
                pl.ds(pl.multiple_of(owner * columns, columns), columns),
            ]
        return wholes[w].at[pl.ds(pl.multiple_of(owner * rows + start, size), size), :]

    def own_piece(item):
        w, cut = item // cuts, item % cuts
        size = locals_[w].shape[0] // (reps * cuts)
        return locals_[w].at[pl.ds(pl.multiple_of((rep * cuts + cut) * size, size), size), :]

    def weight_copy(w, owner, part, slot, device, source=None):
        target = piece(w, owner, part)
        return pltpu.make_async_remote_copy(
            src_ref=target if source is None else source,
            dst_ref=target,
            send_sem=w_send.at[w, owner, slot],
            recv_sem=w_recv.at[w, owner, part],
            device_id=device,
            device_id_type=MESH,
        )

    def own_right(w):
        return weight_copy(w, shard, rep, 0, {"fs": shard + 1}, own_piece(w))

    def own_left(w):
        return weight_copy(w, shard, rep, reps, {"fs": shard - 1}, own_piece(w))

    def send_own(w):
        @pl.when(shard < shards - 1)
        def _():
            own_right(w).start()

        @pl.when(shard > 0)
        def _():
            own_left(w).start()

    def keep_own(w):
        rows, columns = locals_[w].shape
        if side_by_side(w):
            at = pl.ds(pl.multiple_of(shard * columns, columns), columns)
            wholes[w][:, at] = locals_[w][...]
        else:
            wholes[w][pl.ds(pl.multiple_of(shard * rows, rows), rows), :] = locals_[w][...]

    def others(body):
        def at_distance(d, carry):
            for sign in (-1, 1):
                owner = shard + sign * d

                @pl.when((owner >= 0) & (owner < shards))
                def _():
                    body(owner, shard - sign)

            return carry

        lax.fori_loop(1, shards, at_distance, 0)

    def relay(w):
        def body(owner, onward):
            weight_copy(w, owner, rep, 0, partner).wait_recv()

            @pl.when((onward >= 0) & (onward < shards))
            def _():
                weight_copy(w, owner, rep, 0, {"fs": onward}).start()

            for step in range(1, reps):
                weight_copy(w, owner, rep, step, {"rep": lax.rem(rep + step, reps)}).start()

        others(body)

    def arrive(w):
        def body(owner, onward):
            for step in range(1, reps):
                weight_copy(w, owner, lax.rem(rep + step, reps), step, partner).wait_recv()

        others(body)

    def drain(w):
        @pl.when(shard < shards - 1)
        def _():
            own_right(w).wait_send()

        @pl.when(shard > 0)
        def _():
            own_left(w).wait_send()

        def body(owner, onward):
            @pl.when((onward >= 0) & (onward < shards))
            def _():
                weight_copy(w, owner, rep, 0, {"fs": onward}).wait_send()

            for step in range(1, reps):
                weight_copy(
                    w, owner, rep, step, {"rep": lax.rem(rep + step, reps)}
                ).wait_send()

        others(body)

    def position(chip_at, core_at):
        return pl.multiple_of((core_at * chips + chip_at) * block, block)

    strip = block // PARTS

    def row_copy(k, chip_at, core_at, send, part, device, source=None):
        at = pl.multiple_of(position(chip_at, core_at) + part * strip, strip)
        target = rows_all.at[k, pl.ds(at, strip), :]
        return pltpu.make_async_remote_copy(
            src_ref=target if source is None else source.at[pl.ds(part * strip, strip), :],
            dst_ref=target,
            send_sem=send.at[part],
            recv_sem=ag_recv.at[k, core_at * chips + chip_at, part],
            device_id=device,
            device_id_type=MESH,
        )

    def chip_away(step):
        return lax.rem(chip + step, chips)

    def gather_own(k, part, source):
        copies = []
        for step in range(1, chips):
            device = {"tp": chip_away(step) * cores + core}
            copies.append(row_copy(k, chip, core, ag_send.at[k, step], part, device, source))
        if cores > 1:
            copies.append(row_copy(k, chip, core, ag_send.at[k, 0], part, partner, source))
        return copies

    def forward(k, step, part):
        return row_copy(k, chip_away(step), core, fwd_send.at[k, step], part, partner)

    def mirrored(k, step, part):
        return row_copy(
            k, chip_away(step), cores - 1 - core, fwd_send.at[k, step], part, partner
        )

    def gather_start(k, part, source):
        for copy in gather_own(k, part, source):
            copy.start()

    def gathered(k, body):
        if cores > 1:
            for part in range(PARTS):
                mirrored(k, 0, part).wait_recv()

        def at_core(n, carry):
            body(pl.ds(position(chip, n), block))
            return carry

        lax.fori_loop(0, cores, at_core, 0)
        for step in range(1, chips):
            for part in range(PARTS):
                forward(k, step, part).wait_recv()
                if cores > 1:
                    forward(k, step, part).start()

            def at_turn(n, carry):
                @pl.when(n == 1)
                def _():
                    for part in range(PARTS):
                        mirrored(k, step, part).wait_recv()

                turn = jnp.where(n == 0, core, cores - 1 - core)
                body(pl.ds(position(chip_away(step), turn), block))
                return carry

            lax.fori_loop(0, cores, at_turn, 0)

    def part_copy(k, chip_at):
        rows = pl.ds(pl.multiple_of(chip_at * block, block), block)
        return pltpu.make_async_remote_copy(
            src_ref=part_out.at[k, rows, :],
            dst_ref=part_in.at[k, rows, :],
            send_sem=rs_send.at[k, chip_at],
            recv_sem=rs_recv.at[k, lax.rem(chip_at - chip + chips, chips)],
            device_id=partner,
            device_id_type=MESH,
        )

    def cross_copy(k, step, part):
        rows = pl.ds(part * strip, strip)
        return pltpu.make_async_remote_copy(
            src_ref=cross_out.at[k, step - 1, rows, :],
            dst_ref=cross_in.at[k, step - 1, rows, :],
            send_sem=cross_send.at[k, step - 1, part],
            recv_sem=cross_recv.at[k, step - 1, part],
            device_id={"tp": chip_away(step) * cores + core},
            device_id_type=MESH,
        )

    def product(left, weights, core_at, chip_at, into):
        depth, columns = weights.shape[0] // shards, weights.shape[1]
        rows = left[pl.ds(position(chip_at, core_at), block), :]
        to = pl.ds(pl.multiple_of(chip_at * block, block), block)

        def at_shard(j, carry):
            value = dot(rows, weights[pl.ds(pl.multiple_of(j * depth, depth), depth), :])
            into[to, pl.ds(pl.multiple_of(j * columns, columns), columns)] = value.astype(
                into.dtype
            )
            return carry

        lax.fori_loop(0, shards, at_shard, 0)

    def reduce_start(k, left, weights):
        for step in range(1, chips + 1):
            away = chip_away(step)
            if cores > 1:
                product(left, weights, cores - 1 - core, away, part_out.at[k])
                part_copy(k, away).start()
            product(left, weights, core, away, partial)
            if step < chips:
                if cores > 1:
                    part_copy(k, away).wait_recv()
                for part in range(PARTS):
                    rows = pl.ds(pl.multiple_of(away * block + part * strip, strip), strip)
                    value = partial[rows, :]
                    if cores > 1:
                        value = value + part_in[k, rows, :].astype(F32)
                    cross_out[k, step - 1, part * strip : (part + 1) * strip, :] = value.astype(
                        BF16
                    )
                    cross_copy(k, step, part).start()
        if cores > 1:
            part_copy(k, chip).wait_recv()

    chunk = min(32, block)

    def finish_norm(k, part, scale, branch, into, into_start):
        for step in range(1, chips):
            cross_copy(k, step, part).wait_recv()

        def at_chunk(n, carry):
            rows = pl.ds(pl.multiple_of(chip * block + n * chunk, chunk), chunk)
            inner = pl.ds(pl.multiple_of(n * chunk, chunk), chunk)
            summed = partial[rows, :]
            if cores > 1:
                summed = summed + part_in[k, rows, :].astype(F32)
            for step in range(1, chips):
                summed = summed + cross_in[k, step - 1, inner, :].astype(F32)
            current = rows_all[
                k, pl.ds(pl.multiple_of(position(chip, core) + n * chunk, chunk), chunk), :
            ].astype(F32)
            values = RESIDUAL_SCALE * current + (summed if branch == 1.0 else branch * summed)
            centred = values - jnp.mean(values, -1, keepdims=True)
            spread = jnp.mean(centred * centred, -1, keepdims=True)
            done = (centred * lax.rsqrt(spread + NORM_EPS) * scale).astype(BF16)
            into[pl.ds(pl.multiple_of(into_start + n * chunk, chunk), chunk), :] = done
            return carry

        lax.fori_loop(part * strip // chunk, (part + 1) * strip // chunk, at_chunk, 0)

    def norm_to_rows(k, scale, branch):
        for part in range(PARTS):
            finish_norm(k, part, scale, branch, rows_all.at[k + 1], position(chip, core))
            gather_start(k + 1, part, None)

    high = min(256, length)

    def by_rows(body):
        def at_rows(m, carry):
            body(pl.ds(pl.multiple_of(m * high, high), high))
            return carry

        lax.fori_loop(0, length // high, at_rows, 0)

    def silu(values):
        return values / (1.0 + jnp.exp(-values))

    def gate_rows(rows):
        gate_buf[rows, :] = silu(dot(rows_all[0, rows, :], gate_all[...], NT))

    def up_rows(rows):
        upward = dot(rows_all[0, rows, :], up_all[...], NT)
        hidden[rows, :] = (gate_buf[rows, :] * upward).astype(BF16)

    def hidden_rows(rows):
        upward = dot(rows_all[2, rows, :], up_all[...], NT)
        gate = silu(dot(rows_all[2, rows, :], gate_all[...], NT))
        hidden[rows, :] = (gate * upward).astype(BF16)

    keys = decay_up.shape[1]
    heads = keys // DK
    vals = heads * DV

    def project_rows(rows):
        first = rows_all[1, rows, :]
        low = dot(first, decay_down[...], NT).astype(BF16)
        pre = dot(low, decay_up[...]) + decay_bias[...]
        log_gate[rows, :] = (
            jnp.minimum(pre, 0.0) - jnp.log1p(jnp.exp(-jnp.abs(pre)))
        ) / GATE_DIVISOR
        proj[rows, :] = dot(first, qkvg_all[...]).astype(BF16)

    def mix():
        lane_head = lax.broadcasted_iota(jnp.int32, (1, keys), 1) // DK
        lane_masks = [jnp.where(lane_head == h, 1.0, 0.0) for h in range(heads)]
        state[...] = jnp.zeros_like(state)

        def at_tile(n, carry):
            rows = pl.ds(position(n // cores, lax.rem(n, cores)), block)
            query = proj[rows, 0:keys].astype(F32) * DK ** (-0.5)
            key_rows = proj[rows, keys : 2 * keys].astype(F32)
            value_rows = proj[rows, 2 * keys : 2 * keys + vals]
            decay = log_gate[rows, :]
            coarse = decay.astype(BF16)
            fine = (decay - coarse.astype(F32)).astype(BF16)

            def weight(at):
                table = span_sums[at * block : (at + 1) * block, :]
                return jnp.exp(dot(table, coarse) + dot(table, fine))

            scores = [jnp.zeros((block, block), F32) for _ in range(heads)]
            for at in range(levels + 1):
                pairs = pair_masks[at * block : (at + 1) * block, :]
                if at < levels:
                    factor = weight(at)
                    late, early = query * factor, (key_rows * factor).astype(BF16)
                else:
                    late, early = query, key_rows.astype(BF16)
                for h in range(heads):
                    scores[h] = scores[h] + pairs * dot(
                        (late * lane_masks[h]).astype(BF16), early, NT
                    )
            ahead = weight(levels)
            behind = weight(levels + 1)
            late = query * ahead
            held = state[...].astype(BF16)
            for h in range(heads):
                lanes = slice(h * DV, (h + 1) * DV)
                mixed = dot(scores[h].astype(BF16), value_rows[:, lanes]) + dot(
                    (late * lane_masks[h]).astype(BF16), held[lanes, :], NT
                )
                outgate = proj[
                    rows, 2 * keys + vals + h * DV : 2 * keys + vals + (h + 1) * DV
                ].astype(F32)
                normed = (
                    mixed
                    * lax.rsqrt(jnp.mean(mixed * mixed, -1, keepdims=True) + HEAD_EPS)
                    * head_gain[...]
                )
                gated[rows, lanes] = (normed * (outgate / (1.0 + jnp.exp(-outgate)))).astype(BF16)
            state[...] = state[...] * ahead[block - 1 : block, :] + dot(
                value_rows, (key_rows * behind).astype(BF16), TN
            )
            return carry

        lax.fori_loop(0, ranks, at_tile, 0)

    items = len(locals_) * cuts

    def pull(start, stop):
        for item in range(start, stop):
            relay(item)
            if item + AHEAD < items:
                send_own(item + AHEAD)

    def landed(w):
        for item in range(w * cuts, (w + 1) * cuts):
            arrive(item)

    for item in range(min(AHEAD, items)):
        send_own(item)
    for part in range(PARTS):
        gather_start(0, part, stream)
    rows_all[0, pl.ds(position(chip, core), block), :] = stream[...]
    for w in range(len(locals_)):
        keep_own(w)
    pull(0, cuts)
    gathered(0, lambda rows: None)
    pull(cuts, 2 * cuts)
    landed(0)
    by_rows(gate_rows)
    pull(2 * cuts, 3 * cuts)
    landed(1)
    by_rows(up_rows)
    pull(3 * cuts, 3 * cuts + cuts // 2)
    landed(2)
    reduce_start(0, hidden, down_all)
    pull(3 * cuts + cuts // 2, 4 * cuts)
    norm_to_rows(0, norm_gain[0:1, :], BRANCH_SCALE)
    pull(4 * cuts, 5 * cuts)
    landed(3)
    gathered(1, project_rows)
    mix()
    landed(4)
    reduce_start(1, gated, out_all)
    norm_to_rows(1, norm_gain[1:2, :], 1.0)
    gathered(2, hidden_rows)
    reduce_start(2, hidden, down_all)
    for part in range(PARTS):
        finish_norm(2, part, norm_gain[2:3, :], BRANCH_SCALE, result, 0)

    for item in range(items):
        drain(item)
    for k in range(3):
        for part in range(PARTS):
            for copy in gather_own(k, part, stream if k == 0 else None):
                copy.wait_send()
            for step in range(1, chips):
                if cores > 1:
                    forward(k, step, part).wait_send()
                cross_copy(k, step, part).wait_send()
        if cores > 1:
            for chip_at in range(chips):
                part_copy(k, chip_at).wait_send()


def solution(mesh):
    reps, shards, ranks = mesh.shape["rep"], mesh.shape["fs"], mesh.shape["tp"]
    cores = 2 if ranks % 2 == 0 else 1
    chips = ranks // cores

    def on_device(
        stream,
        gate_weight,
        up_weight,
        down_weight,
        query_weight,
        key_weight,
        value_weight,
        outgate_weight,
        decay_down,
        decay_up,
        decay_bias,
        head_gain,
        out_weight,
        norm_gain,
    ):
        qkvg = jnp.concatenate([query_weight, key_weight, value_weight, outgate_weight], axis=1)
        block, width = stream.shape
        length, half_rows = block * ranks, block * chips
        hidden_width = gate_weight.shape[1]
        keys = decay_up.shape[1]
        vals = value_weight.shape[1]
        sums, pairs, levels = level_tables(block)
        vmem = pl.BlockSpec(memory_space=pltpu.VMEM)
        away = max(chips - 1, 1)
        weights = (gate_weight.T, up_weight.T, down_weight, qkvg, out_weight)
        dma = pltpu.SemaphoreType.DMA
        cuts = max(c for c in (1, CUTS) if all(w.shape[0] % (16 * reps * c) == 0 for w in weights))
        return pl.pallas_call(
            functools.partial(layer_kernel, (reps, shards, ranks, cores), levels, cuts),
            out_shape=jax.ShapeDtypeStruct((block, width), BF16),
            in_specs=[vmem] * 13,
            out_specs=vmem,
            scratch_shapes=[
                *[pltpu.VMEM((w.shape[0], shards * w.shape[1]), BF16) for w in weights[:2]],
                *[pltpu.VMEM((shards * w.shape[0], w.shape[1]), BF16) for w in weights[2:]],
                pltpu.VMEM((3, length, width), BF16),
                pltpu.VMEM((3, half_rows, width), BF16),
                pltpu.VMEM((3, half_rows, width), BF16),
                pltpu.VMEM((3, away, block, width), BF16),
                pltpu.VMEM((3, away, block, width), BF16),
                pltpu.VMEM((half_rows, width), F32),
                pltpu.VMEM((length, hidden_width), F32),
                pltpu.VMEM((length, hidden_width), BF16),
                pltpu.VMEM((length, qkvg.shape[1]), BF16),
                pltpu.VMEM((length, keys), F32),
                pltpu.VMEM((length, vals), BF16),
                pltpu.VMEM((vals, keys), F32),
                dma((5 * cuts, shards, reps + 1)),
                dma((5 * cuts, shards, reps)),
                dma((3, chips, PARTS)),
                dma((3, ranks, PARTS)),
                dma((3, chips, PARTS)),
                dma((3, chips)),
                dma((3, chips)),
                dma((3, away, PARTS)),
                dma((3, away, PARTS)),
            ],
            compiler_params=pltpu.CompilerParams(
                collective_id=0, has_side_effects=True, vmem_limit_bytes=60 * 2**20
            ),
            name="layer",
        )(
            stream,
            *weights,
            decay_down.T,
            decay_up,
            decay_bias[None, :],
            head_gain[None, :],
            norm_gain,
            jnp.asarray(sums, BF16),
            jnp.asarray(pairs, F32),
        )

    in_specs = (
        P(("rep", "fs", "tp"), None),
        P("fs", "tp"),
        P("fs", "tp"),
        P("tp", "fs"),
        P("fs", "tp"),
        P("fs", "tp"),
        P("fs", "tp"),
        P("fs", "tp"),
        P(),
        P(None, "tp"),
        P("tp"),
        P(),
        P("tp", "fs"),
        P(),
    )
    return jax.shard_map(
        on_device,
        mesh=mesh,
        in_specs=in_specs,
        out_specs=P(("rep", "fs", "tp"), None),
        check_vma=False,
    )
```

profile of v0, /device:TPU:0, one launch (start us, length us, event | category | flops | bytes accessed | tf_op | source)
XLA Modules:
  0.0 189.8 jit_solution(10822919470987078032)
XLA Ops:
  0.0 2.0 %pad_maximum_fusion.qkvg_w = bf16[512,768]{1,0:T(8,128)(2,1)} fusion(bf16[512,256]{1,0:T(8,128)(2,1)} %param.23, bf16[512,256]{1,0:T(8,128)(2,1)} %param.22, bf16[512,128]{1,0:T(8,128)(2,1)} %param.21, bf16[512,128]{1,0:T(8,128)(2,1)} %param.20), kind=kLoop, calls=%fused_computation | loop fusion | flops 3145728 | bytes 1572864 | tf_op jit(solution)/shard_map/concatenate | solution.py:572
  2.0 185.9 %layer.1 = bf16[128,2048]{1,0:T(8,128)(2,1)} custom-call(bf16[128,2048]{1,0:T(8,128)(2,1)} %stream.1, bf16[704,512]{1,0:T(8,128)(2,1)} %bitcast.5, bf16[704,512]{1,0:T(8,128)(2,1)} %bitcast.6, bf16[704,512]{1,0:T(8,128)(2,1)} %down_w.1, bf16[512,768]{1,0:T(8,128)(2,1)} %pad_maximum_fusion.qkvg_w, bf16[256,512]{1,0:T(8,128)(2,1)} %out_w.1, ...), custom_call_target="tpu_custom_call" | custom-call | tf_op jit(solution)/shard_map/layer/pallas_call | solution.py:584
  187.9 1.9 copy.18
where the time goes:
time: 190 us
  Pallas kernels  186 us (98%)
  other arithmetic  2.04 us (1%)
    pallas_call x1, Pallas kernels, on_device(): pl.pallas_call(functools.partial(layer_kernel, (reps, shards, ranks, core...  186 us

commit v1 on v0

--- a/solution.py
+++ b/solution.py
@@ -18,7 +18,9 @@
 MESH = pl.DeviceIdType.MESH
 CUTS = 2
 AHEAD = 2
-PARTS = 2
+HOST_AHEAD = 2
+PARTS = 4
+HOSTED = 4
 F32 = jnp.float32
 BF16 = jnp.bfloat16
 NT = (((1,), (1,)), ((), ()))
@@ -87,6 +89,7 @@
     log_gate,
     gated,
     state,
+    guest_first,
     w_send,
     w_recv,
     ag_send,
@@ -96,6 +99,10 @@
     rs_recv,
     cross_send,
     cross_recv,
+    guest_send,
+    guest_recv,
+    home_send,
+    home_recv,
 ):
     reps, shards, ranks, cores = sizes
     chips = ranks // cores
@@ -129,6 +136,20 @@
     pl.semaphore_wait(barrier, neighbours)
 
     locals_ = (gate_w, up_w, down_w, qkvg_w, out_w)
+    hosted = shards == HOSTED and cores > 1 and chips > 1
+    guest = 3
+    relayed = 3 * cuts
+    items = len(locals_) * cuts
+    direct = range(cuts // 2, 3 * cuts)
+    at_end = (shard == 0) | (shard == shards - 1)
+    at_host = jnp.logical_not(at_end)
+    near = jnp.where(shard < shards // 2, 0, shards - 1)
+    home = jnp.where(shard < shards // 2, 1, shards - 2)
+    far_host = shards - 1 - shard
+
+    def is_host(at):
+        return (at > 0) & (at < shards - 1)
+
     wholes = (gate_all, up_all, down_all, qkvg_all, out_all)
 
     def side_by_side(w):
@@ -146,10 +167,10 @@
             ]
         return wholes[w].at[pl.ds(pl.multiple_of(owner * rows + start, size), size), :]
 
-    def own_piece(item):
+    def own_piece(item, part=rep):
         w, cut = item // cuts, item % cuts
         size = locals_[w].shape[0] // (reps * cuts)
-        return locals_[w].at[pl.ds(pl.multiple_of((rep * cuts + cut) * size, size), size), :]
+        return locals_[w].at[pl.ds(pl.multiple_of((part * cuts + cut) * size, size), size), :]
 
     def weight_copy(w, owner, part, slot, device, source=None):
         target = piece(w, owner, part)
@@ -177,6 +198,18 @@
         def _():
             own_left(w).start()
 
+    def own_to(item, toward):
+        slot = jnp.where(toward > shard, 0, reps)
+        return weight_copy(item, shard, rep, slot, {"fs": toward}, own_piece(item))
+
+    def own_rest(item):
+        copies = []
+        for step in range(1, reps):
+            part = lax.rem(rep + step, reps)
+            source = own_piece(item, part)
+            copies.append(weight_copy(item, shard, part, step, {"fs": home}, source))
+        return copies
+
     def keep_own(w):
         rows, columns = locals_[w].shape
         if side_by_side(w):
@@ -185,7 +218,7 @@
         else:
             wholes[w][pl.ds(pl.multiple_of(shard * rows, rows), rows), :] = locals_[w][...]
 
-    def others(body):
+    def others(body, nearest=1, furthest=shards - 1):
         def at_distance(d, carry):
             for sign in (-1, 1):
                 owner = shard + sign * d
@@ -196,18 +229,55 @@
 
             return carry
 
-        lax.fori_loop(1, shards, at_distance, 0)
-
-    def relay(w):
+        lax.fori_loop(nearest, furthest + 1, at_distance, 0)
+
+    def onto(item, owner, onward):
+        return weight_copy(item, owner, rep, 0, {"fs": onward})
+
+    def sideways(item, owner):
+        return [
+            weight_copy(item, owner, rep, step, {"rep": lax.rem(rep + step, reps)})
+            for step in range(1, reps)
+        ]
+
+    def relay(item, nearest=1, furthest=shards - 1):
         def body(owner, onward):
-            weight_copy(w, owner, rep, 0, partner).wait_recv()
+            weight_copy(item, owner, rep, 0, partner).wait_recv()
 
             @pl.when((onward >= 0) & (onward < shards))
             def _():
-                weight_copy(w, owner, rep, 0, {"fs": onward}).start()
-
-            for step in range(1, reps):
-                weight_copy(w, owner, rep, step, {"rep": lax.rem(rep + step, reps)}).start()
+                onto(item, owner, onward).start()
+
+            for copy in sideways(item, owner):
+                copy.start()
+
+        others(body, nearest, furthest)
+
+    def relay_from(item, owner, onward):
+        weight_copy(item, owner, rep, 0, partner).wait_recv()
+        onto(item, owner, onward).start()
+        for copy in sideways(item, owner):
+            copy.start()
+
+    def pass_on(item):
+        weight_copy(item, near, rep, 0, partner).wait_recv()
+        onto(item, near, far_host).start()
+        if item not in direct:
+            for copy in sideways(item, near):
+                copy.start()
+        if item + HOST_AHEAD < relayed:
+            own_to(item + HOST_AHEAD, far_host).start()
+
+    def pass_across(item, owner):
+        weight_copy(item, owner, rep, 0, partner).wait_recv()
+        for copy in sideways(item, owner):
+            copy.start()
+
+    def send_late(item):
+        def body(owner, onward):
+            @pl.when(jnp.logical_not(is_host(onward)))
+            def _():
+                onto(item, owner, onward).start()
 
         others(body)
 
@@ -218,24 +288,36 @@
 
         others(body)
 
-    def drain(w):
+    def arrive_from(item, owner):
+        for step in range(1, reps):
+            weight_copy(item, owner, lax.rem(rep + step, reps), step, partner).wait_recv()
+
+    def drain(item):
         @pl.when(shard < shards - 1)
         def _():
-            own_right(w).wait_send()
+            own_right(item).wait_send()
 
         @pl.when(shard > 0)
         def _():
-            own_left(w).wait_send()
+            own_left(item).wait_send()
+
+        first = hosted and item in direct
+        if first:
+
+            @pl.when(at_end)
+            def _():
+                for copy in own_rest(item):
+                    copy.wait_send()
 
         def body(owner, onward):
             @pl.when((onward >= 0) & (onward < shards))
             def _():
-                weight_copy(w, owner, rep, 0, {"fs": onward}).wait_send()
-
-            for step in range(1, reps):
-                weight_copy(
-                    w, owner, rep, step, {"rep": lax.rem(rep + step, reps)}
-                ).wait_send()
+                onto(item, owner, onward).wait_send()
+
+            @pl.when(jnp.logical_not(first & at_host & is_host(onward)))
+            def _():
+                for copy in sideways(item, owner):
+                    copy.wait_send()
 
         others(body)
 
@@ -256,6 +338,28 @@
             device_id_type=MESH,
         )
 
+    def guest_copy(part):
+        at = pl.multiple_of(position(chip, core) + part * strip, strip)
+        return pltpu.make_async_remote_copy(
+            src_ref=stream.at[pl.ds(part * strip, strip), :],
+            dst_ref=rows_all.at[guest, pl.ds(at, strip), :],
+            send_sem=guest_send.at[part],
+            recv_sem=guest_recv.at[part],
+            device_id={"fs": home},
+            device_id_type=MESH,
+        )
+
+    def home_copy(part):
+        at = pl.multiple_of(position(chip, core) + part * strip, strip)
+        return pltpu.make_async_remote_copy(
+            src_ref=guest_first.at[pl.ds(part * strip, strip), :],
+            dst_ref=rows_all.at[1, pl.ds(at, strip), :],
+            send_sem=home_send.at[part],
+            recv_sem=home_recv.at[part],
+            device_id={"fs": near},
+            device_id_type=MESH,
+        )
+
     def chip_away(step):
         return lax.rem(chip + step, chips)
 
@@ -313,8 +417,8 @@
         return pltpu.make_async_remote_copy(
             src_ref=part_out.at[k, rows, :],
             dst_ref=part_in.at[k, rows, :],
-            send_sem=rs_send.at[k, chip_at],
-            recv_sem=rs_recv.at[k, lax.rem(chip_at - chip + chips, chips)],
+            send_sem=rs_send.at[k, chip_at, 0],
+            recv_sem=rs_recv.at[k, lax.rem(chip_at - chip + chips, chips), 0],
             device_id=partner,
             device_id_type=MESH,
         )
@@ -345,18 +449,20 @@
         lax.fori_loop(0, shards, at_shard, 0)
 
     def reduce_start(k, left, weights):
+        sums = partial.at[k // 3]
+
         for step in range(1, chips + 1):
             away = chip_away(step)
             if cores > 1:
                 product(left, weights, cores - 1 - core, away, part_out.at[k])
                 part_copy(k, away).start()
-            product(left, weights, core, away, partial)
+            product(left, weights, core, away, sums)
             if step < chips:
                 if cores > 1:
                     part_copy(k, away).wait_recv()
                 for part in range(PARTS):
                     rows = pl.ds(pl.multiple_of(away * block + part * strip, strip), strip)
-                    value = partial[rows, :]
+                    value = sums[rows, :]
                     if cores > 1:
                         value = value + part_in[k, rows, :].astype(F32)
                     cross_out[k, step - 1, part * strip : (part + 1) * strip, :] = value.astype(
@@ -366,16 +472,100 @@
         if cores > 1:
             part_copy(k, chip).wait_recv()
 
+    depth, columns = locals_[2].shape
+
+    def block_at(chip_at, j):
+        return (
+            pl.ds(pl.multiple_of(chip_at * block, block), block),
+            pl.ds(pl.multiple_of(j * columns, columns), columns),
+        )
+
+    def part_block(k, chip_at, j):
+        at = block_at(chip_at, j)
+        return pltpu.make_async_remote_copy(
+            src_ref=part_out.at[k, at[0], at[1]],
+            dst_ref=part_in.at[k, at[0], at[1]],
+            send_sem=rs_send.at[k, chip_at, j],
+            recv_sem=rs_recv.at[k, lax.rem(chip_at - chip + chips, chips), j],
+            device_id=partner,
+            device_id_type=MESH,
+        )
+
+    def cross_block(k, step, j):
+        at = block_at(0, j)[1]
+        return pltpu.make_async_remote_copy(
+            src_ref=cross_out.at[k, step - 1, :, at],
+            dst_ref=cross_in.at[k, step - 1, :, at],
+            send_sem=cross_send.at[k, step - 1, j],
+            recv_sem=cross_recv.at[k, step - 1, j],
+            device_id={"tp": chip_away(step) * cores + core},
+            device_id_type=MESH,
+        )
+
+    def block_product(k, core_at, chip_at, j):
+        rows = pl.ds(pl.multiple_of(k // 3 * length + position(chip_at, core_at), block), block)
+        return dot(hidden[rows, :], down_all[pl.ds(pl.multiple_of(j * depth, depth), depth), :])
+
+    def block_parts(k, chip_at, j):
+        rows, at = block_at(chip_at, j)
+        part_out[k, rows, at] = block_product(k, cores - 1 - core, chip_at, j).astype(BF16)
+        part_block(k, chip_at, j).start()
+        partial[k // 3, rows, at] = block_product(k, core, chip_at, j)
+
+    def block_cross(k, j):
+        for step in range(1, chips):
+            away = chip_away(step)
+            rows, at = block_at(away, j)
+            part_block(k, away, j).wait_recv()
+            value = partial[k // 3, rows, at] + part_in[k, rows, at].astype(F32)
+            cross_out[k, step - 1, :, at] = value.astype(BF16)
+            cross_block(k, step, j).start()
+
+    def reduce_blocks(owners):
+        for k in (guest, 0):
+            for j in owners:
+                for step in range(1, chips):
+                    block_parts(k, chip_away(step), j)
+            for j in owners:
+                block_cross(k, j)
+
+    def reduce_own(k):
+        def at_shard(j, carry):
+            block_parts(k, chip, j)
+            return carry
+
+        lax.fori_loop(0, shards, at_shard, 0)
+
+    def blocks_landed(k):
+        def at_shard(j, carry):
+            part_block(k, chip, j).wait_recv()
+            for step in range(1, chips):
+                cross_block(k, step, j).wait_recv()
+            return carry
+
+        lax.fori_loop(0, shards, at_shard, 0)
+
+    def drain_blocks(k):
+        def at_shard(j, carry):
+            for chip_at in range(chips):
+                part_block(k, chip_at, j).wait_send()
+            for step in range(1, chips):
+                cross_block(k, step, j).wait_send()
+            return carry
+
+        lax.fori_loop(0, shards, at_shard, 0)
+
     chunk = min(32, block)
 
-    def finish_norm(k, part, scale, branch, into, into_start):
-        for step in range(1, chips):
-            cross_copy(k, step, part).wait_recv()
+    def finish_norm(k, part, scale, branch, into, into_start, blocks=False):
+        if not blocks:
+            for step in range(1, chips):
+                cross_copy(k, step, part).wait_recv()
 
         def at_chunk(n, carry):
             rows = pl.ds(pl.multiple_of(chip * block + n * chunk, chunk), chunk)
             inner = pl.ds(pl.multiple_of(n * chunk, chunk), chunk)
-            summed = partial[rows, :]
+            summed = partial[k // 3, rows, :]
             if cores > 1:
                 summed = summed + part_in[k, rows, :].astype(F32)
             for step in range(1, chips):
@@ -392,9 +582,9 @@
 
         lax.fori_loop(part * strip // chunk, (part + 1) * strip // chunk, at_chunk, 0)
 
-    def norm_to_rows(k, scale, branch):
+    def norm_to_rows(k, scale, branch, blocks=False):
         for part in range(PARTS):
-            finish_norm(k, part, scale, branch, rows_all.at[k + 1], position(chip, core))
+            finish_norm(k, part, scale, branch, rows_all.at[k + 1], position(chip, core), blocks)
             gather_start(k + 1, part, None)
 
     high = min(256, length)
@@ -409,12 +599,20 @@
     def silu(values):
         return values / (1.0 + jnp.exp(-values))
 
-    def gate_rows(rows):
-        gate_buf[rows, :] = silu(dot(rows_all[0, rows, :], gate_all[...], NT))
-
-    def up_rows(rows):
-        upward = dot(rows_all[0, rows, :], up_all[...], NT)
-        hidden[rows, :] = (gate_buf[rows, :] * upward).astype(BF16)
+    def shifted(rows, slot):
+        return pl.ds(pl.multiple_of(rows.start + slot * length, high), high)
+
+    def gate_rows(rows, k=0, slot=0):
+        gate_buf[shifted(rows, slot), :] = silu(dot(rows_all[k, rows, :], gate_all[...], NT))
+
+    def up_rows(rows, k=0, slot=0):
+        upward = dot(rows_all[k, rows, :], up_all[...], NT)
+        at = shifted(rows, slot)
+        hidden[at, :] = (gate_buf[at, :] * upward).astype(BF16)
+
+    def both(rows_body):
+        by_rows(rows_body)
+        by_rows(lambda rows: rows_body(rows, guest, 1))
 
     def hidden_rows(rows):
         upward = dot(rows_all[2, rows, :], up_all[...], NT)
@@ -489,8 +687,6 @@
 
         lax.fori_loop(0, ranks, at_tile, 0)
 
-    items = len(locals_) * cuts
-
     def pull(start, stop):
         for item in range(start, stop):
             relay(item)
@@ -501,51 +697,232 @@
         for item in range(w * cuts, (w + 1) * cuts):
             arrive(item)
 
-    for item in range(min(AHEAD, items)):
-        send_own(item)
-    for part in range(PARTS):
-        gather_start(0, part, stream)
-    rows_all[0, pl.ds(position(chip, core), block), :] = stream[...]
-    for w in range(len(locals_)):
-        keep_own(w)
-    pull(0, cuts)
-    gathered(0, lambda rows: None)
-    pull(cuts, 2 * cuts)
-    landed(0)
-    by_rows(gate_rows)
-    pull(2 * cuts, 3 * cuts)
-    landed(1)
-    by_rows(up_rows)
-    pull(3 * cuts, 3 * cuts + cuts // 2)
-    landed(2)
-    reduce_start(0, hidden, down_all)
-    pull(3 * cuts + cuts // 2, 4 * cuts)
-    norm_to_rows(0, norm_gain[0:1, :], BRANCH_SCALE)
-    pull(4 * cuts, 5 * cuts)
+    own_at = pl.ds(position(chip, core), block)
+
+    def opening():
+        for item in range(min(AHEAD, items)):
+            send_own(item)
+        for part in range(PARTS):
+            gather_start(0, part, stream)
+        rows_all[0, own_at, :] = stream[...]
+        for w in range(len(locals_)):
+            keep_own(w)
+        pull(0, cuts)
+        gathered(0, lambda rows: None)
+        pull(cuts, 2 * cuts)
+        landed(0)
+        by_rows(gate_rows)
+        pull(2 * cuts, 3 * cuts)
+        landed(1)
+        by_rows(up_rows)
+        pull(3 * cuts, 3 * cuts + cuts // 2)
+        landed(2)
+        reduce_start(0, hidden, down_all)
+        pull(3 * cuts + cuts // 2, 4 * cuts)
+        norm_to_rows(0, norm_gain[0:1, :], BRANCH_SCALE)
+        pull(4 * cuts, 5 * cuts)
+
+    def opening_host():
+        for item in range(min(HOST_AHEAD, relayed)):
+            own_to(item, far_host).start()
+        for part in range(PARTS):
+            gather_start(0, part, stream)
+        for item in range(relayed, items):
+            own_to(item, near).start()
+        for item in range(relayed):
+            own_to(item, near).start()
+        rows_all[0, own_at, :] = stream[...]
+        for w in range(len(locals_)):
+            keep_own(w)
+        far_end = shards - 1 - near
+        gates, ups, downs = (range(w * cuts, (w + 1) * cuts) for w in range(3))
+        for item in gates:
+            pass_on(item)
+        for item in gates:
+            pass_across(item, far_host)
+            pass_across(item, far_end)
+        for item in gates:
+            send_late(item)
+        for part in range(PARTS):
+            guest_copy(part).wait_recv()
+            gather_start(guest, part, None)
+        for item in ups:
+            pass_on(item)
+            pass_across(item, far_host)
+            if item == cuts:
+                gathered(0, lambda rows: None)
+            pass_across(item, far_end)
+        for item in ups:
+            onto(item, far_host, near).start()
+        for item in downs:
+            pass_on(item)
+            pass_across(item, far_host)
+        for item in range(relayed, items):
+            own_to(item, far_host).start()
+        gathered(guest, lambda rows: None)
+        landed(0)
+        both(gate_rows)
+        landed(1)
+        both(up_rows)
+        pass_across(2 * cuts, far_end)
+        reduce_blocks([shard])
+        for item in downs[1:]:
+            pass_across(item, far_end)
+        down_items = range(2 * cuts, 3 * cuts)
+        qkvg_items = range(3 * cuts, 4 * cuts)
+        out_items = range(4 * cuts, 5 * cuts)
+        for item in down_items:
+            arrive_from(item, near)
+        reduce_blocks([near])
+        for item in qkvg_items:
+            relay_from(item, far_host, near)
+        for item in down_items:
+            arrive_from(item, far_host)
+            arrive_from(item, far_end)
+        reduce_blocks([far_host, far_end])
+        for item in qkvg_items:
+            relay_from(item, near, far_host)
+        reduce_own(guest)
+        reduce_own(0)
+        blocks_landed(guest)
+        for part in range(PARTS):
+            finish_norm(guest, part, norm_gain[0:1, :], BRANCH_SCALE, guest_first, 0, True)
+            home_copy(part).start()
+        for item in qkvg_items:
+            relay_from(item, far_end, near)
+        for item in out_items:
+            relay_from(item, near, far_host)
+            relay_from(item, far_host, near)
+        blocks_landed(0)
+        norm_to_rows(0, norm_gain[0:1, :], BRANCH_SCALE, True)
+        for item in out_items:
+            relay_from(item, far_end, near)
+        for item in ups:
+            onto(item, far_end, near).start()
+        for item in downs:
+            send_late(item)
+
+    def opening_end():
+        for item in range(cuts):
+            own_to(item, home).start()
+        for part in range(PARTS):
+            guest_copy(part).start()
+        for w in range(3):
+            if w < 2:
+                for item in range((w + 1) * cuts, (w + 2) * cuts):
+                    own_to(item, home).start()
+            for item in range(w * cuts, (w + 1) * cuts):
+                if item in direct:
+                    for copy in own_rest(item):
+                        copy.start()
+        for item in range(relayed, items):
+            own_to(item, home).start()
+        for w in range(len(locals_)):
+            keep_own(w)
+        for item in range(relayed, items):
+            relay(item, 1, 1)
+        for item in range(relayed):
+            relay(item, 1, 1)
+        for item in range(cuts):
+            relay(item, 2)
+        for item in range(cuts, 2 * cuts):
+            relay(item, 2, 2)
+        for item in range(relayed, 4 * cuts):
+            relay(item, 2, 2)
+        for part in range(PARTS):
+            home_copy(part).wait_recv()
+            gather_start(1, part, None)
+        for item in range(relayed, 4 * cuts):
+            relay(item, 3)
+        for item in range(4 * cuts, items):
+            relay(item, 2)
+
+    def late(start, stop, nearest=2):
+        if hosted:
+
+            @pl.when(at_end)
+            def _():
+                for item in range(start, stop):
+                    relay(item, nearest)
+
+    def late_landed(w):
+        if hosted:
+
+            @pl.when(at_end)
+            def _():
+                landed(w)
+
+    if hosted:
+        pl.when(at_host)(opening_host)
+        pl.when(at_end)(opening_end)
+    else:
+        opening()
     landed(3)
     gathered(1, project_rows)
     mix()
+    late(cuts, 2 * cuts, 3)
     landed(4)
     reduce_start(1, gated, out_all)
+    late(2 * cuts, 2 * cuts + 1)
     norm_to_rows(1, norm_gain[1:2, :], 1.0)
+    late(2 * cuts + 1, 3 * cuts)
+    late_landed(0)
+    late_landed(1)
     gathered(2, hidden_rows)
+    late_landed(2)
     reduce_start(2, hidden, down_all)
     for part in range(PARTS):
         finish_norm(2, part, norm_gain[2:3, :], BRANCH_SCALE, result, 0)
 
     for item in range(items):
         drain(item)
-    for k in range(3):
+
+    def drain_rows(k, source=None):
         for part in range(PARTS):
-            for copy in gather_own(k, part, stream if k == 0 else None):
+            for copy in gather_own(k, part, source):
                 copy.wait_send()
             for step in range(1, chips):
                 if cores > 1:
                     forward(k, step, part).wait_send()
+
+    def drain_sums(k):
+        for part in range(PARTS):
+            for step in range(1, chips):
                 cross_copy(k, step, part).wait_send()
         if cores > 1:
             for chip_at in range(chips):
                 part_copy(k, chip_at).wait_send()
+
+    def drain_host():
+        drain_rows(guest)
+        drain_blocks(guest)
+        for part in range(PARTS):
+            home_copy(part).wait_send()
+
+    def drain_end():
+        for part in range(PARTS):
+            guest_copy(part).wait_send()
+
+    def drain_opening():
+        drain_rows(0, stream)
+        if hosted:
+            drain_blocks(0)
+        else:
+            drain_sums(0)
+
+    if hosted:
+
+        @pl.when(at_host)
+        def _():
+            drain_opening()
+            drain_host()
+
+        pl.when(at_end)(drain_end)
+    else:
+        drain_opening()
+    for k in (1, 2):
+        drain_rows(k)
+        drain_sums(k)
 
 
 def solution(mesh):
@@ -578,6 +955,8 @@
         sums, pairs, levels = level_tables(block)
         vmem = pl.BlockSpec(memory_space=pltpu.VMEM)
         away = max(chips - 1, 1)
+        hosted = shards == HOSTED and cores > 1 and chips > 1
+        phases, slots = (4, 2) if hosted else (3, 1)
         weights = (gate_weight.T, up_weight.T, down_weight, qkvg, out_weight)
         dma = pltpu.SemaphoreType.DMA
         cuts = max(c for c in (1, CUTS) if all(w.shape[0] % (16 * reps * c) == 0 for w in weights))
@@ -589,27 +968,29 @@
             scratch_shapes=[
                 *[pltpu.VMEM((w.shape[0], shards * w.shape[1]), BF16) for w in weights[:2]],
                 *[pltpu.VMEM((shards * w.shape[0], w.shape[1]), BF16) for w in weights[2:]],
-                pltpu.VMEM((3, length, width), BF16),
-                pltpu.VMEM((3, half_rows, width), BF16),
-                pltpu.VMEM((3, half_rows, width), BF16),
-                pltpu.VMEM((3, away, block, width), BF16),
-                pltpu.VMEM((3, away, block, width), BF16),
-                pltpu.VMEM((half_rows, width), F32),
-                pltpu.VMEM((length, hidden_width), F32),
-                pltpu.VMEM((length, hidden_width), BF16),
+                pltpu.VMEM((phases, length, width), BF16),
+                pltpu.VMEM((phases, half_rows, width), BF16),
+                pltpu.VMEM((phases, half_rows, width), BF16),
+                pltpu.VMEM((phases, away, block, width), BF16),
+                pltpu.VMEM((phases, away, block, width), BF16),
+                pltpu.VMEM((slots, half_rows, width), F32),
+                pltpu.VMEM((slots * length, hidden_width), F32),
+                pltpu.VMEM((slots * length, hidden_width), BF16),
                 pltpu.VMEM((length, qkvg.shape[1]), BF16),
                 pltpu.VMEM((length, keys), F32),
                 pltpu.VMEM((length, vals), BF16),
                 pltpu.VMEM((vals, keys), F32),
+                pltpu.VMEM((block, width), BF16),
                 dma((5 * cuts, shards, reps + 1)),
                 dma((5 * cuts, shards, reps)),
-                dma((3, chips, PARTS)),
-                dma((3, ranks, PARTS)),
-                dma((3, chips, PARTS)),
-                dma((3, chips)),
-                dma((3, chips)),
-                dma((3, away, PARTS)),
-                dma((3, away, PARTS)),
+                dma((phases, chips, PARTS)),
+                dma((phases, ranks, PARTS)),
+                dma((phases, chips, PARTS)),
+                dma((phases, chips, shards)),
+                dma((phases, chips, shards)),
+                dma((phases, away, max(PARTS, shards))),
+                dma((phases, away, max(PARTS, shards))),
+                *[dma((PARTS,))] * 4,
             ],
             compiler_params=pltpu.CompilerParams(
                 collective_id=0, has_side_effects=True, vmem_limit_bytes=60 * 2**20

time: 190 us -> 179 us (0.942)
  Pallas kernels: 186 us -> 175 us
    pallas_call x1, Pallas kernels: 186 us -> 175 us  [on_device(): pl.pallas_call(functools.partial(layer_kernel, (reps, shards, ranks, core...]
where the time goes in v1:
time: 179 us
  Pallas kernels  175 us (98%)
  other arithmetic  2.04 us (1%)
  local copies, waits for them, and re-layouts  1.88 us (1%)
    pallas_call x1, Pallas kernels, on_device(): pl.pallas_call(functools.partial(layer_kernel, (reps, shards, ranks, core...  175 us

profile of v1, /device:TPU:0, one launch (start us, length us, event | category | flops | bytes accessed | tf_op | source)
XLA Modules:
  0.0 178.6 jit_solution(558280027040765580)
XLA Ops:
  0.0 2.0 %pad_maximum_fusion.qkvg_w = bf16[512,768]{1,0:T(8,128)(2,1)} fusion(bf16[512,256]{1,0:T(8,128)(2,1)} %param.23, bf16[512,256]{1,0:T(8,128)(2,1)} %param.22, bf16[512,128]{1,0:T(8,128)(2,1)} %param.21, bf16[512,128]{1,0:T(8,128)(2,1)} %param.20), kind=kLoop, calls=%fused_computation | loop fusion | flops 3145728 | bytes 1572864 | tf_op jit(solution)/shard_map/concatenate | solution.py:949
  2.0 174.6 %layer.1 = bf16[128,2048]{1,0:T(8,128)(2,1)} custom-call(bf16[128,2048]{1,0:T(8,128)(2,1)} %stream.1, bf16[704,512]{1,0:T(8,128)(2,1)} %bitcast.5, bf16[704,512]{1,0:T(8,128)(2,1)} %bitcast.6, bf16[704,512]{1,0:T(8,128)(2,1)} %down_w.1, bf16[512,768]{1,0:T(8,128)(2,1)} %pad_maximum_fusion.qkvg_w, bf16[256,512]{1,0:T(8,128)(2,1)} %out_w.1, ...), custom_call_target="tpu_custom_call" | custom-call | tf_op jit(solution)/shard_map/layer/pallas_call | solution.py:963
  176.7 1.9 %copy.18 = bf16[128,2048]{1,0:T(8,128)(2,1)} copy(bf16[128,2048]{1,0:T(8,128)(2,1)} %layer.1) | data formatting | bytes 1048576

commit v2 on v1

--- a/solution.py
+++ b/solution.py
@@ -62,7 +62,10 @@
     gate_w,
     up_w,
     down_w,
-    qkvg_w,
+    query_w,
+    key_w,
+    value_w,
+    outgate_w,
     out_w,
     decay_down,
     decay_up,
@@ -90,6 +93,8 @@
     gated,
     state,
     guest_first,
+    qkvg_w,
+    proj_sums,
     w_send,
     w_recv,
     ag_send,
@@ -135,6 +140,11 @@
     )
     pl.semaphore_wait(barrier, neighbours)
 
+    lane = 0
+    for w in (query_w, key_w, value_w, outgate_w):
+        qkvg_w[:, lane : lane + w.shape[1]] = w[...]
+        lane += w.shape[1]
+
     locals_ = (gate_w, up_w, down_w, qkvg_w, out_w)
     hosted = shards == HOSTED and cores > 1 and chips > 1
     guest = 3
@@ -526,8 +536,9 @@
             for j in owners:
                 for step in range(1, chips):
                     block_parts(k, chip_away(step), j)
-            for j in owners:
-                block_cross(k, j)
+            if k == guest:
+                for j in owners:
+                    block_cross(k, j)
 
     def reduce_own(k):
         def at_shard(j, carry):
@@ -555,7 +566,7 @@
 
         lax.fori_loop(0, shards, at_shard, 0)
 
-    chunk = min(32, block)
+    chunk = min(32, strip)
 
     def finish_norm(k, part, scale, branch, into, into_start, blocks=False):
         if not blocks:
@@ -623,14 +634,33 @@
     heads = keys // DK
     vals = heads * DV
 
+    furthest = jnp.where(at_end, shards - 1 - shard, shards - 1 - near)
+
+    def slab(rows, j):
+        deep = qkvg_w.shape[0]
+        at = pl.ds(pl.multiple_of(j * deep, deep), deep)
+        return dot(rows_all[1, rows, at], qkvg_all[at, :])
+
+    def project_most(rows):
+        decay_rows(rows)
+        total = slab(rows, lax.rem(furthest + 1, shards))
+        for step in range(2, shards):
+            total = total + slab(rows, lax.rem(furthest + step, shards))
+        proj_sums[rows, :] = total
+
+    def project_last(rows):
+        proj[rows, :] = (proj_sums[rows, :] + slab(rows, furthest)).astype(BF16)
+
     def project_rows(rows):
-        first = rows_all[1, rows, :]
-        low = dot(first, decay_down[...], NT).astype(BF16)
+        decay_rows(rows)
+        proj[rows, :] = dot(rows_all[1, rows, :], qkvg_all[...]).astype(BF16)
+
+    def decay_rows(rows):
+        low = dot(rows_all[1, rows, :], decay_down[...], NT).astype(BF16)
         pre = dot(low, decay_up[...]) + decay_bias[...]
         log_gate[rows, :] = (
             jnp.minimum(pre, 0.0) - jnp.log1p(jnp.exp(-jnp.abs(pre)))
         ) / GATE_DIVISOR
-        proj[rows, :] = dot(first, qkvg_all[...]).astype(BF16)
 
     def mix():
         lane_head = lax.broadcasted_iota(jnp.int32, (1, keys), 1) // DK
@@ -685,7 +715,7 @@
             )
             return carry
 
-        lax.fori_loop(0, ranks, at_tile, 0)
+        lax.fori_loop(0, ranks, at_tile, 0, unroll=True)
 
     def pull(start, stop):
         for item in range(start, stop):
@@ -748,26 +778,29 @@
             gather_start(guest, part, None)
         for item in ups:
             pass_on(item)
+        for owner in (far_host, far_end):
+            pass_across(cuts, owner)
+        gathered(0, lambda rows: None)
+        for item in downs:
+            pass_on(item)
+        for item in ups[1:]:
             pass_across(item, far_host)
-            if item == cuts:
-                gathered(0, lambda rows: None)
             pass_across(item, far_end)
+        for item in range(relayed, items):
+            own_to(item, far_host).start()
         for item in ups:
             onto(item, far_host, near).start()
-        for item in downs:
-            pass_on(item)
-            pass_across(item, far_host)
-        for item in range(relayed, items):
-            own_to(item, far_host).start()
         gathered(guest, lambda rows: None)
         landed(0)
         both(gate_rows)
+        for item in downs:
+            pass_across(item, far_host)
+        pass_across(2 * cuts, far_end)
         landed(1)
         both(up_rows)
-        pass_across(2 * cuts, far_end)
-        reduce_blocks([shard])
         for item in downs[1:]:
             pass_across(item, far_end)
+        reduce_blocks([shard])
         down_items = range(2 * cuts, 3 * cuts)
         qkvg_items = range(3 * cuts, 4 * cuts)
         out_items = range(4 * cuts, 5 * cuts)
@@ -776,19 +809,23 @@
         reduce_blocks([near])
         for item in qkvg_items:
             relay_from(item, far_host, near)
+        relay_from(3 * cuts, near, far_host)
         for item in down_items:
             arrive_from(item, far_host)
             arrive_from(item, far_end)
         reduce_blocks([far_host, far_end])
-        for item in qkvg_items:
+        for item in qkvg_items[1:]:
             relay_from(item, near, far_host)
+        for j in (shard, near, far_host, far_end):
+            block_cross(0, j)
+        relay_from(3 * cuts, far_end, near)
         reduce_own(guest)
         reduce_own(0)
         blocks_landed(guest)
         for part in range(PARTS):
             finish_norm(guest, part, norm_gain[0:1, :], BRANCH_SCALE, guest_first, 0, True)
             home_copy(part).start()
-        for item in qkvg_items:
+        for item in qkvg_items[1:]:
             relay_from(item, far_end, near)
         for item in out_items:
             relay_from(item, near, far_host)
@@ -807,14 +844,11 @@
             own_to(item, home).start()
         for part in range(PARTS):
             guest_copy(part).start()
-        for w in range(3):
-            if w < 2:
-                for item in range((w + 1) * cuts, (w + 2) * cuts):
-                    own_to(item, home).start()
-            for item in range(w * cuts, (w + 1) * cuts):
-                if item in direct:
-                    for copy in own_rest(item):
-                        copy.start()
+        for item in range(cuts, relayed):
+            own_to(item, home).start()
+        for item in direct:
+            for copy in own_rest(item):
+                copy.start()
         for item in range(relayed, items):
             own_to(item, home).start()
         for w in range(len(locals_)):
@@ -829,13 +863,12 @@
             relay(item, 2, 2)
         for item in range(relayed, 4 * cuts):
             relay(item, 2, 2)
+        relay(3 * cuts, 3)
         for part in range(PARTS):
             home_copy(part).wait_recv()
             gather_start(1, part, None)
-        for item in range(relayed, 4 * cuts):
+        for item in range(3 * cuts + 1, 4 * cuts):
             relay(item, 3)
-        for item in range(4 * cuts, items):
-            relay(item, 2)
 
     def late(start, stop, nearest=2):
         if hosted:
@@ -857,8 +890,23 @@
         pl.when(at_end)(opening_end)
     else:
         opening()
-    landed(3)
-    gathered(1, project_rows)
+    if hosted:
+        for item in range(3 * cuts, 4 * cuts):
+            for step in range(1, shards):
+                owner = lax.rem(furthest + step, shards)
+
+                @pl.when(owner != shard)
+                def _():
+                    arrive_from(item, owner)
+
+        gathered(1, project_most)
+        for item in range(3 * cuts, 4 * cuts):
+            arrive_from(item, furthest)
+        by_rows(project_last)
+    else:
+        landed(3)
+        gathered(1, project_rows)
+    late(4 * cuts, items)
     mix()
     late(cuts, 2 * cuts, 3)
     landed(4)
@@ -871,9 +919,6 @@
     gathered(2, hidden_rows)
     late_landed(2)
     reduce_start(2, hidden, down_all)
-    for part in range(PARTS):
-        finish_norm(2, part, norm_gain[2:3, :], BRANCH_SCALE, result, 0)
-
     for item in range(items):
         drain(item)
 
@@ -920,9 +965,12 @@
         pl.when(at_end)(drain_end)
     else:
         drain_opening()
-    for k in (1, 2):
-        drain_rows(k)
-        drain_sums(k)
+    drain_rows(1)
+    drain_sums(1)
+    drain_rows(2)
+    for part in range(PARTS):
+        finish_norm(2, part, norm_gain[2:3, :], BRANCH_SCALE, result, 0)
+    drain_sums(2)
 
 
 def solution(mesh):
@@ -946,7 +994,8 @@
         out_weight,
         norm_gain,
     ):
-        qkvg = jnp.concatenate([query_weight, key_weight, value_weight, outgate_weight], axis=1)
+        projections = (query_weight, key_weight, value_weight, outgate_weight)
+        qkvg = jax.ShapeDtypeStruct((query_weight.shape[0], sum(w.shape[1] for w in projections)), BF16)
         block, width = stream.shape
         length, half_rows = block * ranks, block * chips
         hidden_width = gate_weight.shape[1]
@@ -963,7 +1012,7 @@
         return pl.pallas_call(
             functools.partial(layer_kernel, (reps, shards, ranks, cores), levels, cuts),
             out_shape=jax.ShapeDtypeStruct((block, width), BF16),
-            in_specs=[vmem] * 13,
+            in_specs=[vmem] * 16,
             out_specs=vmem,
             scratch_shapes=[
                 *[pltpu.VMEM((w.shape[0], shards * w.shape[1]), BF16) for w in weights[:2]],
@@ -981,6 +1030,8 @@
                 pltpu.VMEM((length, vals), BF16),
                 pltpu.VMEM((vals, keys), F32),
                 pltpu.VMEM((block, width), BF16),
+                pltpu.VMEM(qkvg.shape, BF16),
+                pltpu.VMEM((length, qkvg.shape[1]), F32),
                 dma((5 * cuts, shards, reps + 1)),
                 dma((5 * cuts, shards, reps)),
                 dma((phases, chips, PARTS)),
@@ -998,7 +1049,9 @@
             name="layer",
         )(
             stream,
-            *weights,
+            *weights[:3],
+            *projections,
+            out_weight,
             decay_down.T,
             decay_up,
             decay_bias[None, :],

time: 179 us -> 166 us (0.927)
  Pallas kernels: 175 us -> 164 us
  other arithmetic: 2.04 us -> 0 us
    pallas_call x1, Pallas kernels: 175 us -> 164 us  [on_device(): pl.pallas_call(functools.partial(layer_kernel, (reps, shards, ranks, core...]
    concatenate x1 -> x0, other arithmetic: 2.04 us -> none  [on_device(): jnp.concatenate([query_weight, key_weight, value_weight, outgate_weight],...]
where the time goes in v2:
time: 166 us
  Pallas kernels  164 us (99%)
  local copies, waits for them, and re-layouts  1.88 us (1%)
    pallas_call x1, Pallas kernels, on_device(): pl.pallas_call(functools.partial(layer_kernel, (reps, shards, ranks, core...  164 us

profile of v2, /device:TPU:0, one launch (start us, length us, event | category | flops | bytes accessed | tf_op | source)
XLA Modules:
  0.0 165.5 jit_solution(12732886341222178505)
XLA Ops:
  0.0 163.6 %layer.1 = bf16[128,2048]{1,0:T(8,128)(2,1)} custom-call(bf16[128,2048]{1,0:T(8,128)(2,1)} %stream.1, bf16[704,512]{1,0:T(8,128)(2,1)} %bitcast.5, bf16[704,512]{1,0:T(8,128)(2,1)} %bitcast.6, bf16[704,512]{1,0:T(8,128)(2,1)} %down_w.1, bf16[512,128]{1,0:T(8,128)(2,1)} %query_w.1, bf16[512,128]{1,0:T(8,128)(2,1)} %key_w.1, bf16[512,256]{1,0:T(8,128)(2,1)} %value_w.1, ...), custom_call_target="tpu_custom_call" | custom-call | tf_op jit(solution)/shard_map/layer/pallas_call | solution.py:1012
  163.7 1.9 %copy.18 = bf16[128,2048]{1,0:T(8,128)(2,1)} copy(bf16[128,2048]{1,0:T(8,128)(2,1)} %layer.1) | data formatting | bytes 1048576

commit v3 on v2

--- a/solution.py
+++ b/solution.py
@@ -95,6 +95,8 @@
     guest_first,
     qkvg_w,
     proj_sums,
+    decays,
+    factors,
     w_send,
     w_recv,
     ag_send,
@@ -336,8 +338,16 @@
 
     strip = block // PARTS
 
+    fold = 2 if hosted else 1
+    lap = block // fold
+
+    def row_at(k, chip_at, core_at, offset):
+        if k != 2:
+            return position(chip_at, core_at) + offset
+        return (chip_at * fold + offset // lap) * cores * lap + core_at * lap + offset % lap
+
     def row_copy(k, chip_at, core_at, send, part, device, source=None):
-        at = pl.multiple_of(position(chip_at, core_at) + part * strip, strip)
+        at = pl.multiple_of(row_at(k, chip_at, core_at, part * strip), strip)
         target = rows_all.at[k, pl.ds(at, strip), :]
         return pltpu.make_async_remote_copy(
             src_ref=target if source is None else source.at[pl.ds(part * strip, strip), :],
@@ -400,7 +410,7 @@
                 mirrored(k, 0, part).wait_recv()
 
         def at_core(n, carry):
-            body(pl.ds(position(chip, n), block))
+            body(pl.ds(pl.multiple_of(row_at(k, chip, n, 0), block), block))
             return carry
 
         lax.fori_loop(0, cores, at_core, 0)
@@ -417,7 +427,7 @@
                         mirrored(k, step, part).wait_recv()
 
                 turn = jnp.where(n == 0, core, cores - 1 - core)
-                body(pl.ds(position(chip_away(step), turn), block))
+                body(pl.ds(pl.multiple_of(row_at(k, chip_away(step), turn, 0), block), block))
                 return carry
 
             lax.fori_loop(0, cores, at_turn, 0)
@@ -444,9 +454,10 @@
             device_id_type=MESH,
         )
 
-    def product(left, weights, core_at, chip_at, into):
+    def product(k, left, weights, core_at, chip_at, into):
         depth, columns = weights.shape[0] // shards, weights.shape[1]
-        rows = left[pl.ds(position(chip_at, core_at), block), :]
+        at = row_at(k, chip_at, core_at, 0)
+        rows = left[pl.ds(pl.multiple_of(at, block), block), :]
         to = pl.ds(pl.multiple_of(chip_at * block, block), block)
 
         def at_shard(j, carry):
@@ -464,9 +475,9 @@
         for step in range(1, chips + 1):
             away = chip_away(step)
             if cores > 1:
-                product(left, weights, cores - 1 - core, away, part_out.at[k])
+                product(k, left, weights, cores - 1 - core, away, part_out.at[k])
                 part_copy(k, away).start()
-            product(left, weights, core, away, sums)
+            product(k, left, weights, core, away, sums)
             if step < chips:
                 if cores > 1:
                     part_copy(k, away).wait_recv()
@@ -531,12 +542,12 @@
             cross_out[k, step - 1, :, at] = value.astype(BF16)
             cross_block(k, step, j).start()
 
-    def reduce_blocks(owners):
+    def reduce_blocks(owners, early=False):
         for k in (guest, 0):
             for j in owners:
                 for step in range(1, chips):
                     block_parts(k, chip_away(step), j)
-            if k == guest:
+            if k == guest or early:
                 for j in owners:
                     block_cross(k, j)
 
@@ -566,9 +577,75 @@
 
         lax.fori_loop(0, shards, at_shard, 0)
 
+    def part_lap(chip_at, h):
+        rows = pl.ds(pl.multiple_of(chip_at * block + h * lap, lap), lap)
+        return pltpu.make_async_remote_copy(
+            src_ref=part_out.at[2, rows, :],
+            dst_ref=part_in.at[2, rows, :],
+            send_sem=rs_send.at[2, chip_at, h],
+            recv_sem=rs_recv.at[2, lax.rem(chip_at - chip + chips, chips), h],
+            device_id=partner,
+            device_id_type=MESH,
+        )
+
+    def lap_product(core_at, chip_at, h, into):
+        left = pl.ds(pl.multiple_of(row_at(2, chip_at, core_at, h * lap), lap), lap)
+        to = pl.ds(pl.multiple_of(chip_at * block + h * lap, lap), lap)
+
+        def at_shard(j, carry):
+            value = dot(hidden[left, :], down_all[pl.ds(pl.multiple_of(j * depth, depth), depth), :])
+            into[to, pl.ds(pl.multiple_of(j * columns, columns), columns)] = value.astype(into.dtype)
+            return carry
+
+        lax.fori_loop(0, shards, at_shard, 0)
+
+    def lap_parts(chip_at, h):
+        lap_product(cores - 1 - core, chip_at, h, part_out.at[2])
+        part_lap(chip_at, h).start()
+        lap_product(core, chip_at, h, partial.at[0])
+
+    def second_block():
+        per_lap = PARTS // fold
+        for part in range(PARTS):
+            mirrored(2, 0, part).wait_recv()
+        hidden_rows(pl.ds(pl.multiple_of(chip * cores * block, cores * block), cores * block))
+        for h in range(fold):
+            parts = range(h * per_lap, (h + 1) * per_lap)
+            for step in range(1, chips):
+                for part in parts:
+                    forward(2, step, part).wait_recv()
+                    forward(2, step, part).start()
+            for step in range(1, chips):
+                away = chip_away(step)
+                for part in parts:
+                    mirrored(2, step, part).wait_recv()
+                at = (away * fold + h) * cores * lap
+                hidden_rows(pl.ds(pl.multiple_of(at, cores * lap), cores * lap))
+                if h == 0:
+                    late_landed(2)
+                lap_parts(away, h)
+                part_lap(away, h).wait_recv()
+                for part in parts:
+                    rows = pl.ds(pl.multiple_of(away * block + part * strip, strip), strip)
+                    value = partial[0, rows, :] + part_in[2, rows, :].astype(F32)
+                    cross_out[2, step - 1, part * strip : (part + 1) * strip, :] = value.astype(BF16)
+                    cross_copy(2, step, part).start()
+        for h in range(fold):
+            lap_parts(chip, h)
+        for h in range(fold):
+            part_lap(chip, h).wait_recv()
+
+    def drain_laps():
+        for h in range(fold):
+            for chip_at in range(chips):
+                part_lap(chip_at, h).wait_send()
+        for part in range(PARTS):
+            for step in range(1, chips):
+                cross_copy(2, step, part).wait_send()
+
     chunk = min(32, strip)
 
-    def finish_norm(k, part, scale, branch, into, into_start, blocks=False):
+    def finish_norm(k, part, scale, branch, into, into_at, blocks=False):
         if not blocks:
             for step in range(1, chips):
                 cross_copy(k, step, part).wait_recv()
@@ -582,20 +659,25 @@
             for step in range(1, chips):
                 summed = summed + cross_in[k, step - 1, inner, :].astype(F32)
             current = rows_all[
-                k, pl.ds(pl.multiple_of(position(chip, core) + n * chunk, chunk), chunk), :
+                k, pl.ds(pl.multiple_of(row_at(k, chip, core, n * chunk), chunk), chunk), :
             ].astype(F32)
             values = RESIDUAL_SCALE * current + (summed if branch == 1.0 else branch * summed)
             centred = values - jnp.mean(values, -1, keepdims=True)
             spread = jnp.mean(centred * centred, -1, keepdims=True)
             done = (centred * lax.rsqrt(spread + NORM_EPS) * scale).astype(BF16)
-            into[pl.ds(pl.multiple_of(into_start + n * chunk, chunk), chunk), :] = done
+            into[pl.ds(pl.multiple_of(into_at(n * chunk), chunk), chunk), :] = done
             return carry
 
         lax.fori_loop(part * strip // chunk, (part + 1) * strip // chunk, at_chunk, 0)
 
-    def norm_to_rows(k, scale, branch, blocks=False):
+    def norm_to_rows(k, scale, branch, blocks=False, meanwhile=None):
         for part in range(PARTS):
-            finish_norm(k, part, scale, branch, rows_all.at[k + 1], position(chip, core), blocks)
+            if meanwhile is not None and part == 1:
+                meanwhile()
+            finish_norm(
+                k, part, scale, branch, rows_all.at[k + 1],
+                lambda offset: row_at(k + 1, chip, core, offset), blocks,
+            )
             gather_start(k + 1, part, None)
 
     high = min(256, length)
@@ -661,6 +743,24 @@
         log_gate[rows, :] = (
             jnp.minimum(pre, 0.0) - jnp.log1p(jnp.exp(-jnp.abs(pre)))
         ) / GATE_DIVISOR
+
+    bulk = keys % 128 == 0
+
+    def spread():
+        for n in range(ranks):
+            rows = pl.ds(position(n // cores, n % cores), block)
+            decay = log_gate[rows, :]
+            coarse = decay.astype(BF16)
+            lanes = slice(n * keys, (n + 1) * keys)
+            decays[0:block, lanes] = coarse
+            decays[block : 2 * block, lanes] = (decay - coarse.astype(F32)).astype(BF16)
+
+        def at_table(at, carry):
+            rows = pl.ds(pl.multiple_of(at * block, block), block)
+            factors[rows, :] = jnp.exp(dot(span_sums[rows, :], decays[...]))
+            return carry
+
+        lax.fori_loop(0, levels + 2, at_table, 0)
 
     def mix():
         lane_head = lax.broadcasted_iota(jnp.int32, (1, keys), 1) // DK
@@ -677,7 +777,10 @@
             fine = (decay - coarse.astype(F32)).astype(BF16)
 
             def weight(at):
-                table = span_sums[at * block : (at + 1) * block, :]
+                if bulk:
+                    lanes = pl.ds(pl.multiple_of(n * keys, keys), keys)
+                    return factors[at * block : (at + 1) * block, lanes]
+                table = span_sums[at * block : (at + 1) * block, 0:block]
                 return jnp.exp(dot(table, coarse) + dot(table, fine))
 
             scores = [jnp.zeros((block, block), F32) for _ in range(heads)]
@@ -800,14 +903,14 @@
         both(up_rows)
         for item in downs[1:]:
             pass_across(item, far_end)
-        reduce_blocks([shard])
+        reduce_blocks([shard], True)
         down_items = range(2 * cuts, 3 * cuts)
         qkvg_items = range(3 * cuts, 4 * cuts)
         out_items = range(4 * cuts, 5 * cuts)
         for item in down_items:
             arrive_from(item, near)
         reduce_blocks([near])
-        for item in qkvg_items:
+        for item in (*qkvg_items, *out_items):
             relay_from(item, far_host, near)
         relay_from(3 * cuts, near, far_host)
         for item in down_items:
@@ -816,20 +919,19 @@
         reduce_blocks([far_host, far_end])
         for item in qkvg_items[1:]:
             relay_from(item, near, far_host)
-        for j in (shard, near, far_host, far_end):
+        for j in (near, far_host, far_end):
             block_cross(0, j)
         relay_from(3 * cuts, far_end, near)
         reduce_own(guest)
         reduce_own(0)
         blocks_landed(guest)
         for part in range(PARTS):
-            finish_norm(guest, part, norm_gain[0:1, :], BRANCH_SCALE, guest_first, 0, True)
+            finish_norm(guest, part, norm_gain[0:1, :], BRANCH_SCALE, guest_first, lambda offset: offset, True)
             home_copy(part).start()
         for item in qkvg_items[1:]:
             relay_from(item, far_end, near)
         for item in out_items:
             relay_from(item, near, far_host)
-            relay_from(item, far_host, near)
         blocks_landed(0)
         norm_to_rows(0, norm_gain[0:1, :], BRANCH_SCALE, True)
         for item in out_items:
@@ -863,6 +965,8 @@
             relay(item, 2, 2)
         for item in range(relayed, 4 * cuts):
             relay(item, 2, 2)
+        for item in range(4 * cuts, items):
+            relay(item, 2, 2)
         relay(3 * cuts, 3)
         for part in range(PARTS):
             home_copy(part).wait_recv()
@@ -900,25 +1004,33 @@
                     arrive_from(item, owner)
 
         gathered(1, project_most)
+        if bulk:
+            spread()
+        late(4 * cuts, items, 3)
         for item in range(3 * cuts, 4 * cuts):
             arrive_from(item, furthest)
         by_rows(project_last)
     else:
         landed(3)
         gathered(1, project_rows)
-    late(4 * cuts, items)
+        if bulk:
+            spread()
     mix()
-    late(cuts, 2 * cuts, 3)
+    late(cuts, cuts + 1, 3)
     landed(4)
+    late(cuts + 1, 2 * cuts, 3)
     reduce_start(1, gated, out_all)
-    late(2 * cuts, 2 * cuts + 1)
-    norm_to_rows(1, norm_gain[1:2, :], 1.0)
+    norm_to_rows(
+        1, norm_gain[1:2, :], 1.0, meanwhile=lambda: late(2 * cuts, 2 * cuts + 1)
+    )
     late(2 * cuts + 1, 3 * cuts)
     late_landed(0)
     late_landed(1)
-    gathered(2, hidden_rows)
-    late_landed(2)
-    reduce_start(2, hidden, down_all)
+    if hosted:
+        second_block()
+    else:
+        gathered(2, hidden_rows)
+        reduce_start(2, hidden, down_all)
     for item in range(items):
         drain(item)
 
@@ -969,8 +1081,11 @@
     drain_sums(1)
     drain_rows(2)
     for part in range(PARTS):
-        finish_norm(2, part, norm_gain[2:3, :], BRANCH_SCALE, result, 0)
-    drain_sums(2)
+        finish_norm(2, part, norm_gain[2:3, :], BRANCH_SCALE, result, lambda offset: offset)
+    if hosted:
+        drain_laps()
+    else:
+        drain_sums(2)
 
 
 def solution(mesh):
@@ -1032,6 +1147,8 @@
                 pltpu.VMEM((block, width), BF16),
                 pltpu.VMEM(qkvg.shape, BF16),
                 pltpu.VMEM((length, qkvg.shape[1]), F32),
+                pltpu.VMEM((2 * block, ranks * keys), BF16),
+                pltpu.VMEM(((levels + 2) * block, ranks * keys), F32),
                 dma((5 * cuts, shards, reps + 1)),
                 dma((5 * cuts, shards, reps)),
                 dma((phases, chips, PARTS)),
@@ -1057,7 +1174,7 @@
             decay_bias[None, :],
             head_gain[None, :],
             norm_gain,
-            jnp.asarray(sums, BF16),
+            jnp.asarray(np.concatenate([sums, sums], 1), BF16),
             jnp.asarray(pairs, F32),
         )
 

time: 166 us -> 157 us (0.946)
  Pallas kernels: 164 us -> 155 us
    pallas_call x1, Pallas kernels: 164 us -> 155 us  [on_device(): pl.pallas_call(functools.partial(layer_kernel, (reps, shards, ranks, core...]
where the time goes in v3:
time: 157 us
  Pallas kernels  155 us (99%)
  local copies, waits for them, and re-layouts  1.88 us (1%)
    pallas_call x1, Pallas kernels, on_device(): pl.pallas_call(functools.partial(layer_kernel, (reps, shards, ranks, core...  155 us

profile of v3, /device:TPU:0, one launch (start us, length us, event | category | flops | bytes accessed | tf_op | source)
XLA Modules:
  0.0 156.9 jit_solution(11908548703050217723)
XLA Ops:
  0.0 155.0 %layer.1 = bf16[128,2048]{1,0:T(8,128)(2,1)} custom-call(bf16[128,2048]{1,0:T(8,128)(2,1)} %stream.1, bf16[704,512]{1,0:T(8,128)(2,1)} %bitcast.5, bf16[704,512]{1,0:T(8,128)(2,1)} %bitcast.6, bf16[704,512]{1,0:T(8,128)(2,1)} %down_w.1, bf16[512,128]{1,0:T(8,128)(2,1)} %query_w.1, bf16[512,128]{1,0:T(8,128)(2,1)} %key_w.1, bf16[512,256]{1,0:T(8,128)(2,1)} %value_w.1, ...), custom_call_target="tpu_custom_call" | custom-call | tf_op jit(solution)/shard_map/layer/pallas_call | solution.py:1127
  155.0 1.9 %copy.18 = bf16[128,2048]{1,0:T(8,128)(2,1)} copy(bf16[128,2048]{1,0:T(8,128)(2,1)} %layer.1) | data formatting | bytes 1048576

commit v4 on v3

--- a/solution.py
+++ b/solution.py
@@ -58,6 +58,7 @@
     sizes,
     levels,
     cuts,
+    finer,
     stream,
     gate_w,
     up_w,
@@ -140,18 +141,21 @@
     neighbours = (
         jnp.where(shard > 0, 1, 0) + jnp.where(shard < shards - 1, 1, 0) + reps - 1 + ranks - 1
     )
-    pl.semaphore_wait(barrier, neighbours)
-
     lane = 0
     for w in (query_w, key_w, value_w, outgate_w):
         qkvg_w[:, lane : lane + w.shape[1]] = w[...]
         lane += w.shape[1]
 
+    pl.semaphore_wait(barrier, neighbours)
+
     locals_ = (gate_w, up_w, down_w, qkvg_w, out_w)
     hosted = shards == HOSTED and cores > 1 and chips > 1
     guest = 3
-    relayed = 3 * cuts
-    items = len(locals_) * cuts
+    counts = (cuts, cuts, cuts, cuts * finer, cuts)
+    starts = [sum(counts[:w]) for w in range(len(counts) + 1)]
+    places = [(w, cut) for w in range(len(counts)) for cut in range(counts[w])]
+    relayed = starts[3]
+    items = starts[5]
     direct = range(cuts // 2, 3 * cuts)
     at_end = (shard == 0) | (shard == shards - 1)
     at_host = jnp.logical_not(at_end)
@@ -168,10 +172,10 @@
         return wholes[w].shape[0] == locals_[w].shape[0]
 
     def piece(item, owner, part):
-        w, cut = item // cuts, item % cuts
+        w, cut = places[item]
         rows, columns = locals_[w].shape
-        size = rows // (reps * cuts)
-        start = (part * cuts + cut) * size
+        size = rows // (reps * counts[w])
+        start = (part * counts[w] + cut) * size
         if side_by_side(w):
             return wholes[w].at[
                 pl.ds(pl.multiple_of(start, size), size),
@@ -180,9 +184,10 @@
         return wholes[w].at[pl.ds(pl.multiple_of(owner * rows + start, size), size), :]
 
     def own_piece(item, part=rep):
-        w, cut = item // cuts, item % cuts
-        size = locals_[w].shape[0] // (reps * cuts)
-        return locals_[w].at[pl.ds(pl.multiple_of((part * cuts + cut) * size, size), size), :]
+        w, cut = places[item]
+        size = locals_[w].shape[0] // (reps * counts[w])
+        start = pl.multiple_of((part * counts[w] + cut) * size, size)
+        return locals_[w].at[pl.ds(start, size), :]
 
     def weight_copy(w, owner, part, slot, device, source=None):
         target = piece(w, owner, part)
@@ -405,6 +410,10 @@
             copy.start()
 
     def gathered(k, body):
+        gathered_near(k, body)
+        gathered_away(k, body)
+
+    def gathered_near(k, body):
         if cores > 1:
             for part in range(PARTS):
                 mirrored(k, 0, part).wait_recv()
@@ -414,6 +423,8 @@
             return carry
 
         lax.fori_loop(0, cores, at_core, 0)
+
+    def gathered_away(k, body):
         for step in range(1, chips):
             for part in range(PARTS):
                 forward(k, step, part).wait_recv()
@@ -467,7 +478,7 @@
             )
             return carry
 
-        lax.fori_loop(0, shards, at_shard, 0)
+        lax.fori_loop(0, shards, at_shard, 0, unroll=hosted)
 
     def reduce_start(k, left, weights):
         sums = partial.at[k // 3]
@@ -597,7 +608,7 @@
             into[to, pl.ds(pl.multiple_of(j * columns, columns), columns)] = value.astype(into.dtype)
             return carry
 
-        lax.fori_loop(0, shards, at_shard, 0)
+        lax.fori_loop(0, shards, at_shard, 0, unroll=True)
 
     def lap_parts(chip_at, h):
         lap_product(cores - 1 - core, chip_at, h, part_out.at[2])
@@ -672,8 +683,8 @@
 
     def norm_to_rows(k, scale, branch, blocks=False, meanwhile=None):
         for part in range(PARTS):
-            if meanwhile is not None and part == 1:
-                meanwhile()
+            if meanwhile is not None:
+                meanwhile(part)
             finish_norm(
                 k, part, scale, branch, rows_all.at[k + 1],
                 lambda offset: row_at(k + 1, chip, core, offset), blocks,
@@ -746,21 +757,23 @@
 
     bulk = keys % 128 == 0
 
-    def spread():
-        for n in range(ranks):
-            rows = pl.ds(position(n // cores, n % cores), block)
+    def spread(chip_at):
+        span = cores * keys
+        for n in range(cores):
+            rows = pl.ds(position(chip_at, n), block)
             decay = log_gate[rows, :]
             coarse = decay.astype(BF16)
             lanes = slice(n * keys, (n + 1) * keys)
             decays[0:block, lanes] = coarse
             decays[block : 2 * block, lanes] = (decay - coarse.astype(F32)).astype(BF16)
+        across = pl.ds(pl.multiple_of(chip_at * span, span), span)
 
         def at_table(at, carry):
             rows = pl.ds(pl.multiple_of(at * block, block), block)
-            factors[rows, :] = jnp.exp(dot(span_sums[rows, :], decays[...]))
+            factors[rows, across] = jnp.exp(dot(span_sums[rows, :], decays[...]))
             return carry
 
-        lax.fori_loop(0, levels + 2, at_table, 0)
+        lax.fori_loop(0, levels + 2, at_table, 0, unroll=True)
 
     def mix():
         lane_head = lax.broadcasted_iota(jnp.int32, (1, keys), 1) // DK
@@ -827,7 +840,7 @@
                 send_own(item + AHEAD)
 
     def landed(w):
-        for item in range(w * cuts, (w + 1) * cuts):
+        for item in range(starts[w], starts[w + 1]):
             arrive(item)
 
     own_at = pl.ds(position(chip, core), block)
@@ -848,12 +861,12 @@
         pull(2 * cuts, 3 * cuts)
         landed(1)
         by_rows(up_rows)
-        pull(3 * cuts, 3 * cuts + cuts // 2)
+        pull(relayed, relayed + counts[3] // 2)
         landed(2)
         reduce_start(0, hidden, down_all)
-        pull(3 * cuts + cuts // 2, 4 * cuts)
+        pull(relayed + counts[3] // 2, starts[4])
         norm_to_rows(0, norm_gain[0:1, :], BRANCH_SCALE)
-        pull(4 * cuts, 5 * cuts)
+        pull(starts[4], items)
 
     def opening_host():
         for item in range(min(HOST_AHEAD, relayed)):
@@ -868,12 +881,13 @@
         for w in range(len(locals_)):
             keep_own(w)
         far_end = shards - 1 - near
-        gates, ups, downs = (range(w * cuts, (w + 1) * cuts) for w in range(3))
+        gates, ups, downs = (range(starts[w], starts[w + 1]) for w in range(3))
         for item in gates:
             pass_on(item)
+            pass_across(item, far_host)
         for item in gates:
-            pass_across(item, far_host)
             pass_across(item, far_end)
+        pass_across(cuts, far_host)
         for item in gates:
             send_late(item)
         for part in range(PARTS):
@@ -881,8 +895,7 @@
             gather_start(guest, part, None)
         for item in ups:
             pass_on(item)
-        for owner in (far_host, far_end):
-            pass_across(cuts, owner)
+        pass_across(cuts, far_end)
         gathered(0, lambda rows: None)
         for item in downs:
             pass_on(item)
@@ -905,30 +918,33 @@
             pass_across(item, far_end)
         reduce_blocks([shard], True)
         down_items = range(2 * cuts, 3 * cuts)
-        qkvg_items = range(3 * cuts, 4 * cuts)
-        out_items = range(4 * cuts, 5 * cuts)
+        qkvg_items = range(relayed, starts[4])
+        out_items = range(starts[4], items)
         for item in down_items:
             arrive_from(item, near)
-        reduce_blocks([near])
+        reduce_blocks([near], True)
         for item in (*qkvg_items, *out_items):
             relay_from(item, far_host, near)
-        relay_from(3 * cuts, near, far_host)
+        half = relayed + (starts[4] - relayed) // 2
+        for item in range(relayed, half):
+            relay_from(item, near, far_host)
         for item in down_items:
             arrive_from(item, far_host)
             arrive_from(item, far_end)
         reduce_blocks([far_host, far_end])
-        for item in qkvg_items[1:]:
+        for item in range(half, starts[4]):
             relay_from(item, near, far_host)
-        for j in (near, far_host, far_end):
+        for j in (far_host, far_end):
             block_cross(0, j)
-        relay_from(3 * cuts, far_end, near)
+        for item in range(relayed, half):
+            relay_from(item, far_end, near)
         reduce_own(guest)
         reduce_own(0)
         blocks_landed(guest)
         for part in range(PARTS):
             finish_norm(guest, part, norm_gain[0:1, :], BRANCH_SCALE, guest_first, lambda offset: offset, True)
             home_copy(part).start()
-        for item in qkvg_items[1:]:
+        for item in range(half, starts[4]):
             relay_from(item, far_end, near)
         for item in out_items:
             relay_from(item, near, far_host)
@@ -963,16 +979,16 @@
             relay(item, 2)
         for item in range(cuts, 2 * cuts):
             relay(item, 2, 2)
-        for item in range(relayed, 4 * cuts):
+        for item in range(relayed, starts[4]):
             relay(item, 2, 2)
-        for item in range(4 * cuts, items):
+        for item in range(starts[4], items):
             relay(item, 2, 2)
-        relay(3 * cuts, 3)
+        half = relayed + (starts[4] - relayed) // 2
+        for item in range(relayed, half):
+            relay(item, 3)
         for part in range(PARTS):
             home_copy(part).wait_recv()
             gather_start(1, part, None)
-        for item in range(3 * cuts + 1, 4 * cuts):
-            relay(item, 3)
 
     def late(start, stop, nearest=2):
         if hosted:
@@ -988,6 +1004,12 @@
             @pl.when(at_end)
             def _():
                 landed(w)
+
+    def late_downs(part):
+        if part == 1:
+            late(2 * cuts, 2 * cuts + 1)
+        if part == PARTS - 1:
+            late(2 * cuts + 1, 3 * cuts)
 
     if hosted:
         pl.when(at_host)(opening_host)
@@ -995,7 +1017,7 @@
     else:
         opening()
     if hosted:
-        for item in range(3 * cuts, 4 * cuts):
+        for item in range(relayed, starts[4]):
             for step in range(1, shards):
                 owner = lax.rem(furthest + step, shards)
 
@@ -1003,27 +1025,34 @@
                 def _():
                     arrive_from(item, owner)
 
-        gathered(1, project_most)
+        gathered_near(1, project_most)
+        half = relayed + (starts[4] - relayed) // 2
+        late(half, starts[4] - 1, 3)
         if bulk:
-            spread()
-        late(4 * cuts, items, 3)
-        for item in range(3 * cuts, 4 * cuts):
+            spread(chip)
+        late(max(half, starts[4] - 1), starts[4], 3)
+        gathered_away(1, project_most)
+        late(starts[4], items, 3)
+        if bulk:
+            for step in range(1, chips):
+                spread(chip_away(step))
+        for item in range(relayed, starts[4]):
             arrive_from(item, furthest)
         by_rows(project_last)
     else:
         landed(3)
         gathered(1, project_rows)
         if bulk:
-            spread()
+            for step in range(1, chips + 1):
+                spread(chip_away(step))
     mix()
     late(cuts, cuts + 1, 3)
     landed(4)
+    reduce_start(1, gated, out_all)
     late(cuts + 1, 2 * cuts, 3)
-    reduce_start(1, gated, out_all)
     norm_to_rows(
-        1, norm_gain[1:2, :], 1.0, meanwhile=lambda: late(2 * cuts, 2 * cuts + 1)
+        1, norm_gain[1:2, :], 1.0, meanwhile=late_downs
     )
-    late(2 * cuts + 1, 3 * cuts)
     late_landed(0)
     late_landed(1)
     if hosted:
@@ -1124,8 +1153,10 @@
         weights = (gate_weight.T, up_weight.T, down_weight, qkvg, out_weight)
         dma = pltpu.SemaphoreType.DMA
         cuts = max(c for c in (1, CUTS) if all(w.shape[0] % (16 * reps * c) == 0 for w in weights))
+        finer = 2 if hosted and qkvg.shape[0] % (32 * reps * cuts) == 0 else 1
+        pieces = cuts * (4 + finer)
         return pl.pallas_call(
-            functools.partial(layer_kernel, (reps, shards, ranks, cores), levels, cuts),
+            functools.partial(layer_kernel, (reps, shards, ranks, cores), levels, cuts, finer),
             out_shape=jax.ShapeDtypeStruct((block, width), BF16),
             in_specs=[vmem] * 16,
             out_specs=vmem,
@@ -1147,10 +1178,10 @@
                 pltpu.VMEM((block, width), BF16),
                 pltpu.VMEM(qkvg.shape, BF16),
                 pltpu.VMEM((length, qkvg.shape[1]), F32),
-                pltpu.VMEM((2 * block, ranks * keys), BF16),
+                pltpu.VMEM((2 * block, cores * keys), BF16),
                 pltpu.VMEM(((levels + 2) * block, ranks * keys), F32),
-                dma((5 * cuts, shards, reps + 1)),
-                dma((5 * cuts, shards, reps)),
+                dma((pieces, shards, reps + 1)),
+                dma((pieces, shards, reps)),
                 dma((phases, chips, PARTS)),
                 dma((phases, ranks, PARTS)),
                 dma((phases, chips, PARTS)),

time: 157 us -> 154 us (0.981)
  Pallas kernels: 155 us -> 152 us
    pallas_call x1, Pallas kernels: 155 us -> 152 us  [on_device(): pl.pallas_call(functools.partial(layer_kernel, (reps, shards, ranks, core...]
where the time goes in v4:
time: 154 us; the launch traced here: 153 us
  Pallas kernels  152 us (99%)
  local copies, waits for them, and re-layouts  1.88 us (1%)
    pallas_call x1, Pallas kernels, on_device(): pl.pallas_call(functools.partial(layer_kernel, (reps, shards, ranks, core...  152 us

profile of v4, /device:TPU:0, one launch (start us, length us, event | category | flops | bytes accessed | tf_op | source)
XLA Modules:
  0.0 153.5 jit_solution(2243695873454255958)
XLA Ops:
  0.0 151.6 %layer.1 = bf16[128,2048]{1,0:T(8,128)(2,1)} custom-call(bf16[128,2048]{1,0:T(8,128)(2,1)} %stream.1, bf16[704,512]{1,0:T(8,128)(2,1)} %bitcast.5, bf16[704,512]{1,0:T(8,128)(2,1)} %bitcast.6, bf16[704,512]{1,0:T(8,128)(2,1)} %down_w.1, bf16[512,128]{1,0:T(8,128)(2,1)} %query_w.1, bf16[512,128]{1,0:T(8,128)(2,1)} %key_w.1, bf16[512,256]{1,0:T(8,128)(2,1)} %value_w.1, ...), custom_call_target="tpu_custom_call" | custom-call | tf_op jit(solution)/shard_map/layer/pallas_call | solution.py:1158
  151.6 1.9 %copy.18 = bf16[128,2048]{1,0:T(8,128)(2,1)} copy(bf16[128,2048]{1,0:T(8,128)(2,1)} %layer.1) | data formatting | bytes 1048576
